TPU v7x, 32 devices: a whole 2x2x4 slice. The times are simulated.
32 devices in a mesh: grp: 2 (over y), sp: 4 (over z), tp: 4 (over x, core).
Axes of the slice: x: 2, y: 2, z: 4, core: 2. Of those that a mesh axis runs over, the one named last changes fastest.
Arguments:
- stream: bfloat16 [2048, 2048], P(('grp', 'sp'), 'tp'), parts along dimension 0, may hold values from -1.5 to 1.5
- layer_norm_gain: float32 [2, 2048], replicated, may hold values from 0.1 to 1.9
- convolution_in_weight: bfloat16 [2, 2048, 1536], P(None, 'sp', 'tp'), may hold values from -0.125 to 0.125
- gating_in_weight: bfloat16 [2, 2048, 1536], P(None, 'sp', 'tp'), may hold values from -0.125 to 0.125
- output_weight: bfloat16 [2, 1536, 2048], P(None, 'tp', 'sp'), may hold values from -0.15625 to 0.15625
- convolution_kernel_taps: float32 [2, 4, 1536], P(None, None, 'tp'), may hold values from -12 to 12
- recurrent_gate_blocks: bfloat16 [2, 2, 2, 12, 128, 128], P(None, None, None, 'tp'), may hold values from -0.5 to 0.5
- channel_decay_logit: float32 [2, 2, 1536], P(None, None, 'tp')
- position_decay_boost: float32 [2, 2, 2048], P(None, None, ('grp', 'sp')), parts along dimension 2, may hold values from -1.4 to 0, as said below
Outputs:
- new_stream: bfloat16 [2048, 2048], P(('grp', 'sp'), 'tp'), parts along dimension 0
There are 2 independent parts, one for each index of `grp`. A program takes and returns all parts, laid end to end along the dimension named above; an argument that names none is the same for every part. Nothing has to cross between parts.
Inputs may be any that keep to these rules, and one draw needn't show every extreme that they name: `position_decay_boost`: zero at all but a few positions.
All inputs are finite; a program needn't handle non-finite values.
Results may differ from a plain program's by a relative error of at most 0.025.
Values may be sent and summed in bfloat16 or wider, within the bound.
A program may use at most 128 MiB of HBM per device.

v0:
```python
import jax
import jax.numpy as jnp
from jax import lax
from jax.sharding import PartitionSpec as P

EPS = 1e-06
RECURRENT_WIDTH = 8.0


def extended(cells, sides, width):
    for axis, dim in sides:
        count = lax.axis_size(axis)
        ends = count - 1
        head = lax.slice_in_dim(cells, 0, width, axis=dim)
        tail = lax.slice_in_dim(cells, cells.shape[dim] - width, cells.shape[dim], axis=dim)
        cells = jnp.concatenate(
            [
                lax.ppermute(tail, axis, [(i, (i + 1) % count) for i in range(ends)]),
                cells,
                lax.ppermute(head, axis, [((i + 1) % count, i) for i in range(ends)]),
            ],
            axis=dim,
        )
    return cells


def carried_in(part, axis, combine, identity, reverse):
    count = lax.axis_size(axis)
    place = lax.axis_index(axis)
    ahead = count - 1 - place if reverse else place
    gathered = jax.tree.map(lambda a: lax.all_gather(a, axis), part)
    state = jax.tree.map(lambda a, e: jnp.zeros_like(a) + jnp.asarray(e, a.dtype), part, identity)

    def one(step, state):
        source = count - 1 - step if reverse else step
        return combine(
            state, jax.tree.map(lambda a: lax.dynamic_index_in_dim(a, source, 0, False), gathered)
        )

    return lax.fori_loop(0, ahead, one, state)


def rms_norm(values, gain_row):
    floats = values.astype(jnp.float32)
    inverse = lax.rsqrt(jnp.mean(floats * floats, axis=-1, keepdims=True) + EPS)
    return (floats * inverse * gain_row).astype(jnp.bfloat16)


def combine_pairs(earlier, latter):
    return (earlier[0] * latter[0], latter[0] * earlier[1] + latter[1])


def local(
    stream,
    layer_norm_gain,
    convolution_in_weight,
    gating_in_weight,
    output_weight,
    convolution_kernel_taps,
    recurrent_gate_blocks,
    channel_decay_logit,
    position_decay_boost,
):
    tok_rows = stream.shape[0]
    channels = convolution_in_weight.shape[2]
    gate_count = recurrent_gate_blocks.shape[3]
    block_width = recurrent_gate_blocks.shape[4]
    seq_devices = lax.axis_size("sp")
    my_index = lax.axis_index("sp")
    seq_length = tok_rows * seq_devices
    positions = my_index * tok_rows + lax.iota(jnp.int32, tok_rows)
    at_first = (positions == 0)[:, None]
    at_last = (positions == seq_length - 1)[:, None]
    for layer_index in range(convolution_in_weight.shape[0]):
        features = lax.all_gather(stream, "tp", axis=1, tiled=True)
        normed = rms_norm(features, layer_norm_gain[layer_index])
        acc_x = jnp.dot(
            normed,
            lax.all_gather(convolution_in_weight[layer_index], "sp", axis=0, tiled=True),
            preferred_element_type=jnp.float32,
        )
        acc_y = jnp.dot(
            normed,
            lax.all_gather(gating_in_weight[layer_index], "sp", axis=0, tiled=True),
            preferred_element_type=jnp.float32,
        )
        proj_x = acc_x.astype(jnp.bfloat16)
        proj_y = acc_y.astype(jnp.bfloat16)
        padded = extended(proj_x, (("sp", 0),), 2).astype(jnp.float32)
        taps_now = convolution_kernel_taps[layer_index]
        conv_mixed = (
            taps_now[0] * padded[1 : tok_rows + 1]
            + taps_now[1] * padded[2 : tok_rows + 2]
            + taps_now[2] * padded[3 : tok_rows + 3]
            + taps_now[3] * padded[4 : tok_rows + 4]
        )
        convolution_output = conv_mixed.astype(jnp.bfloat16)
        conv_float = convolution_output.astype(jnp.float32)
        grouped = convolution_output.reshape(tok_rows, gate_count, block_width)
        results = []
        for scan_direction in range(2):
            gate_matrix_pair = recurrent_gate_blocks[layer_index, scan_direction]
            recurrent_branch = jax.nn.sigmoid(
                jnp.einsum(
                    "tnc,ncd->tnd", grouped, gate_matrix_pair[0], preferred_element_type=jnp.float32
                ).reshape(tok_rows, channels)
            )
            input_gate = jax.nn.sigmoid(
                jnp.einsum(
                    "tnc,ncd->tnd", grouped, gate_matrix_pair[1], preferred_element_type=jnp.float32
                ).reshape(tok_rows, channels)
            )
            decay_logarithm = (
                -RECURRENT_WIDTH
                * jax.nn.softplus(-channel_decay_logit[layer_index, scan_direction])
                * recurrent_branch
                + position_decay_boost[layer_index, scan_direction][:, None]
            )
            is_start = at_first if scan_direction == 0 else at_last
            multiplier = jnp.where(is_start, 1.0, jnp.sqrt(-jnp.expm1(2.0 * decay_logarithm)))
            driven = multiplier * input_gate * conv_float
            results.append(
                lax.associative_scan(
                    combine_pairs,
                    (jnp.exp(decay_logarithm), driven),
                    reverse=scan_direction == 1,
                    axis=0,
                )
            )
        cum_fwd, local_fwd = results[0]
        cum_bwd, local_bwd = results[1]
        identity = (jnp.ones((1, channels), jnp.float32), jnp.zeros((1, channels), jnp.float32))
        enter_fwd = carried_in(
            (cum_fwd[-1:], local_fwd[-1:]), "sp", combine_pairs, identity, False
        )[1]
        enter_bwd = carried_in((cum_bwd[:1], local_bwd[:1]), "sp", combine_pairs, identity, True)[1]
        state_sum = local_fwd + cum_fwd * enter_fwd + local_bwd + cum_bwd * enter_bwd
        gated = (state_sum * jax.nn.gelu(proj_y.astype(jnp.float32))).astype(jnp.bfloat16)
        partials = jnp.dot(
            gated,
            lax.all_gather(output_weight[layer_index], "sp", axis=1, tiled=True),
            preferred_element_type=jnp.float32,
        ).astype(jnp.bfloat16)
        branch_sum = lax.psum_scatter(
            partials.astype(jnp.float32).astype(jnp.bfloat16), "tp", scatter_dimension=1, tiled=True
        ).astype(jnp.float32)
        stream = (stream.astype(jnp.float32) + branch_sum).astype(jnp.bfloat16)
    return stream


def solution(mesh):
    return jax.shard_map(
        local,
        mesh=mesh,
        in_specs=(
            P(("grp", "sp"), "tp"),
            P(),
            P(None, "sp", "tp"),
            P(None, "sp", "tp"),
            P(None, "tp", "sp"),
            P(None, None, "tp"),
            P(None, None, None, "tp", None, None),
            P(None, None, "tp"),
            P(None, None, ("grp", "sp")),
        ),
        out_specs=P(("grp", "sp"), "tp"),
        check_vma=False,
    )
```

profile of v0, /device:TPU:0, one launch (start us, length us, event | category | flops | bytes accessed | tf_op | source)
XLA Modules:
  0.0 358.1 jit_solution(14976978191996592059)
XLA Ops:
  6.5 0.7 all-gather.31.cloned.1.call-update
  7.3 2.1 fusion.206
  9.5 1.0 fusion.207
  10.7 0.9 fusion.208
  15.3 13.0 %all-gather.31.cloned.1.call-done = bf16[256,2048]{1,0:T(8,128)(2,1)} async-done(((bf16[256,512]{1,0:T(8,128)(2,1)}), bf16[256,2048]{1,0:T(8,128)(2,1)}) %all-gather.31.cloned.1.call-update) | async-done | bytes 1048592 | tf_op jit(solution)/shard_map/all_gather | solution.py:75
  28.3 1.5 fusion
  29.9 37.1 %all-gather.35.cloned.1.call-done = bf16[1,2048,384]{2,1,0:T(8,128)(2,1)} async-done(((bf16[1,512,384]{2,1,0:T(8,128)(2,1)}), bf16[1,2048,384]{2,1,0:T(8,128)(2,1)}) %all-gather.35.cloned.1.call-update) | async-done | bytes 1572880 | tf_op jit(solution)/shard_map/all_gather | solution.py:79
  67.0 2.5 fusion.40
  69.5 2.6 collective-permute-start
  72.1 1.3 collective-permute-start.1
  73.5 4.2 %collective-permute-done.1 = bf16[2,384]{1,0:T(2,128)(2,1)S(1)} collective-permute-done((bf16[2,384]{1,0:T(2,128)(2,1)S(1)}, bf16[2,384]{1,0:T(2,128)(2,1)S(1)}, u32[]{:S(2)}, u32[]{:S(2)}) %collective-permute-start.1) | collective-permute-done | bytes 1568 | tf_op jit(solution)/shard_map/ppermute | solution.py:20
  80.0 1.6 convert_multiply_fusion.7
  87.3 12.3 %all-gather.15 = f32[4,1,384]{2,1,0:T(1,128)S(1)} all-gather(f32[1,1,384]{2,1,0:T(1,128)S(1)} %add_bitcast_fusion.6), channel_id=4, replica_groups=mesh['grp'=2,'sp'=4,'tp'=4] {'sp'}, dimensions={0}, use_global_device_ids=true | all-gather | bytes 7680 | tf_op jit(solution)/shard_map/all_gather | solution.py:31
  99.7 11.9 %all-gather.14 = f32[4,1,384]{2,1,0:T(1,128)S(1)} all-gather(f32[1,1,384]{2,1,0:T(1,128)S(1)} %add_bitcast_fusion.7), channel_id=3, replica_groups=mesh['grp'=2,'sp'=4,'tp'=4] {'sp'}, dimensions={0}, use_global_device_ids=true | all-gather | bytes 7680 | tf_op jit(solution)/shard_map/all_gather | solution.py:31
  116.5 1.6 pad.454
  118.1 0.8 add.988
  118.9 1.9 add.997
  120.8 0.7 add_bitcast_fusion.4
  121.5 12.5 %all-gather.17 = f32[4,1,384]{2,1,0:T(1,128)S(1)} all-gather(f32[1,1,384]{2,1,0:T(1,128)S(1)} %add_bitcast_fusion.4), channel_id=6, replica_groups=mesh['grp'=2,'sp'=4,'tp'=4] {'sp'}, dimensions={0}, use_global_device_ids=true | all-gather | bytes 7680 | tf_op jit(solution)/shard_map/all_gather | solution.py:31
  134.0 0.7 add_bitcast_fusion.5
  134.7 12.1 %all-gather.16 = f32[4,1,384]{2,1,0:T(1,128)S(1)} all-gather(f32[1,1,384]{2,1,0:T(1,128)S(1)} %add_bitcast_fusion.5), channel_id=5, replica_groups=mesh['grp'=2,'sp'=4,'tp'=4] {'sp'}, dimensions={0}, use_global_device_ids=true | all-gather | bytes 7680 | tf_op jit(solution)/shard_map/all_gather | solution.py:31
  146.9 2.6 rev.16
  149.5 2.6 rev.17
  152.2 4.4 %convolution_convert_fusion.1 = bf16[256,2048]{1,0:T(8,128)(2,1)} fusion(bf16[1,384,2048]{2,1,0:T(8,128)(2,1)} %all-gather.39.cloned.1.call-done, bf16[1,2048,384]{2,1,0:T(8,128)(2,1)} %all-gather.37.cloned.1.call-done, f32[256,384]{1,0:T(8,128)S(1)} %rev.17, f32[256,384]{1,0:T(8,128)S(1)} %rev.16, f32[256,384]{1,0:T(8,128)S(1)} %pad.422, ...), kind=kOutput, calls=%fused_computation.13 | convolution fusion | flops 809795584 | bytes 7614464 | tf_op jit(solution)/shard_map/dot_general | solution.py:139
  156.9 22.8 %reduce-scatter.3.cloned.1.call-done = bf16[256,512]{1,0:T(8,128)(2,1)} async-done(((bf16[256,2048]{1,0:T(8,128)(2,1)}), bf16[256,512]{1,0:T(8,128)(2,1)}) %reduce-scatter.3.cloned.1.call-update) | async-done | bytes 262160 | tf_op jit(solution)/shard_map/reduce_scatter | solution.py:144
  179.6 1.8 add_convert_fusion.1
  184.4 13.9 %all-gather.33.cloned.1.call-done = bf16[256,2048]{1,0:T(8,128)(2,1)} async-done(((bf16[256,512]{1,0:T(8,128)(2,1)}), bf16[256,2048]{1,0:T(8,128)(2,1)}) %all-gather.33.cloned.1.call-update) | async-done | bytes 1048592 | tf_op jit(solution)/shard_map/all_gather | solution.py:75
  198.3 1.5 fusion.3
  199.8 37.1 %all-gather.41.cloned.1.call-done = bf16[1,2048,384]{2,1,0:T(8,128)(2,1)} async-done(((bf16[1,512,384]{2,1,0:T(8,128)(2,1)}), bf16[1,2048,384]{2,1,0:T(8,128)(2,1)}) %all-gather.41.cloned.1.call-update) | async-done | bytes 1572880 | tf_op jit(solution)/shard_map/all_gather | solution.py:79
  236.9 2.5 fusion.49
  239.5 2.6 collective-permute-start.2
  242.1 1.3 collective-permute-start.3
  243.4 4.2 %collective-permute-done.3 = bf16[2,384]{1,0:T(2,128)(2,1)S(1)} collective-permute-done((bf16[2,384]{1,0:T(2,128)(2,1)S(1)}, bf16[2,384]{1,0:T(2,128)(2,1)S(1)}, u32[]{:S(2)}, u32[]{:S(2)}) %collective-permute-start.3) | collective-permute-done | bytes 1568 | tf_op jit(solution)/shard_map/ppermute | solution.py:20
  250.0 1.6 convert_multiply_fusion.5
  257.2 12.3 %all-gather.19 = f32[4,1,384]{2,1,0:T(1,128)S(1)} all-gather(f32[1,1,384]{2,1,0:T(1,128)S(1)} %add_bitcast_fusion.2), channel_id=11, replica_groups=mesh['grp'=2,'sp'=4,'tp'=4] {'sp'}, dimensions={0}, use_global_device_ids=true | all-gather | bytes 7680 | tf_op jit(solution)/shard_map/all_gather | solution.py:31
  269.7 11.9 %all-gather.18 = f32[4,1,384]{2,1,0:T(1,128)S(1)} all-gather(f32[1,1,384]{2,1,0:T(1,128)S(1)} %add_bitcast_fusion.3), channel_id=10, replica_groups=mesh['grp'=2,'sp'=4,'tp'=4] {'sp'}, dimensions={0}, use_global_device_ids=true | all-gather | bytes 7680 | tf_op jit(solution)/shard_map/all_gather | solution.py:31
  284.9 1.6 pad.518
  286.5 0.8 add.1076
  287.4 1.9 add.1085
  289.2 0.7 add_bitcast_fusion
  289.9 12.4 %all-gather.21 = f32[4,1,384]{2,1,0:T(1,128)S(1)} all-gather(f32[1,1,384]{2,1,0:T(1,128)S(1)} %add_bitcast_fusion), channel_id=13, replica_groups=mesh['grp'=2,'sp'=4,'tp'=4] {'sp'}, dimensions={0}, use_global_device_ids=true | all-gather | bytes 7680 | tf_op jit(solution)/shard_map/all_gather | solution.py:31
  302.3 0.7 add_bitcast_fusion.1
  303.0 12.1 %all-gather.20 = f32[4,1,384]{2,1,0:T(1,128)S(1)} all-gather(f32[1,1,384]{2,1,0:T(1,128)S(1)} %add_bitcast_fusion.1), channel_id=12, replica_groups=mesh['grp'=2,'sp'=4,'tp'=4] {'sp'}, dimensions={0}, use_global_device_ids=true | all-gather | bytes 7680 | tf_op jit(solution)/shard_map/all_gather | solution.py:31
  315.2 2.6 rev.18
  317.8 3.9 %rev.19 = f32[256,384]{1,0:T(8,128)} reverse(f32[256,384]{1,0:T(8,128)} %add.1085), dimensions={0} | reverse | bytes 786432 | tf_op jit(solution)/shard_map/rev | solution.py:123
  321.7 4.6 %convolution_convert_fusion = bf16[256,2048]{1,0:T(8,128)(2,1)} fusion(bf16[1,384,2048]{2,1,0:T(8,128)(2,1)} %all-gather.45.cloned.1.call-done, bf16[1,2048,384]{2,1,0:T(8,128)(2,1)} %all-gather.43.cloned.1.call-done, f32[256,384]{1,0:T(8,128)} %rev.19, f32[256,384]{1,0:T(8,128)S(1)} %rev.18, f32[256,384]{1,0:T(8,128)S(1)} %pad.486, ...), kind=kOutput, calls=%fused_computation.12 | convolution fusion | flops 809795584 | bytes 7614464 | tf_op jit(solution)/shard_map/dot_general | solution.py:139
  326.3 23.2 %reduce-scatter.5.cloned.1.call-done = bf16[256,512]{1,0:T(8,128)(2,1)} async-done(((bf16[256,2048]{1,0:T(8,128)(2,1)}), bf16[256,512]{1,0:T(8,128)(2,1)}) %reduce-scatter.5.cloned.1.call-update) | async-done | bytes 262160 | tf_op jit(solution)/shard_map/reduce_scatter | solution.py:144
  349.5 1.7 add_convert_fusion
  (646 shorter events, 29.0 us)
Async XLA Ops:
  6.5 2.9 copy-start.5
  6.5 21.8 %all-gather.31.cloned.1.call-start = ((), (), s32[]{:S(2)}) async-start(), calls=%async_computation.2 | async-start | bytes 1310720 | tf_op jit(solution)/shard_map/all_gather | solution.py:75
  7.3 59.7 %all-gather.35.cloned.1.call-start = ((), (), s32[]{:S(2)}) async-start(), calls=%async_computation.6 | async-start | bytes 1966080 | tf_op jit(solution)/shard_map/all_gather | solution.py:79
  9.4 1.3 copy-start.6
  9.4 142.7 %all-gather.37.cloned.1.call-start = ((), (), s32[]{:S(2)}) async-start(), calls=%async_computation.7 | async-start | bytes 1966080 | tf_op jit(solution)/shard_map/all_gather | solution.py:84
  10.4 1.2 copy-start.18
  10.4 1.8 copy-start.19
  10.4 2.5 copy-start.24
  10.4 3.7 %copy-start.29 = (f32[2,2,256]{2,1,0:T(2,128)S(1)}, f32[2,2,256]{2,1,0:T(2,128)}, u32[]{:S(2)}) copy-start(f32[2,2,256]{2,1,0:T(2,128)} %param.25) | copy-start | bytes 12292
  10.5 141.7 %all-gather.39.cloned.1.call-start = ((), (), s32[]{:S(2)}) async-start(), calls=%async_computation.8 | async-start | bytes 1966080 | tf_op jit(solution)/shard_map/all_gather | solution.py:141
  11.6 168.0 %reduce-scatter.3.cloned.1.call-start = ((), (), s32[]{:S(2)}) async-start(), calls=%async_computation.3 | async-start | bytes 1310720 | tf_op jit(solution)/shard_map/reduce_scatter | solution.py:144
  12.3 57.2 %copy-start.9 = (f32[1,2048]{1,0:T(1,128)}, f32[1,2048]{1,0:T(1,128)S(1)}, u32[]{:S(2)}) copy-start(f32[1,2048]{1,0:T(1,128)S(1)} %get-tuple-element.404) | copy-start | bytes 24580
  12.9 64.7 %copy-start.14 = (f32[384]{0:T(512)}, f32[384]{0:T(512)S(1)}, u32[]{:S(2)}) copy-start(f32[384]{0:T(512)S(1)} %get-tuple-element.267) | copy-start | bytes 4612
  12.9 64.7 %copy-start.15 = (f32[384]{0:T(512)}, f32[384]{0:T(512)S(1)}, u32[]{:S(2)}) copy-start(f32[384]{0:T(512)S(1)} %get-tuple-element.268) | copy-start | bytes 4612
  12.9 64.7 %copy-start.16 = (f32[384]{0:T(512)}, f32[384]{0:T(512)S(1)}, u32[]{:S(2)}) copy-start(f32[384]{0:T(512)S(1)} %get-tuple-element.269) | copy-start | bytes 4612
  12.9 64.8 %copy-start.17 = (f32[384]{0:T(512)}, f32[384]{0:T(512)S(1)}, u32[]{:S(2)}) copy-start(f32[384]{0:T(512)S(1)} %get-tuple-element.270) | copy-start | bytes 4612
  29.9 39.6 %copy-start.27 = (f32[256]{0:T(256)}, f32[256]{0:T(256)S(1)}, u32[]{:S(2)}) copy-start(f32[256]{0:T(256)S(1)} %add_rsqrt_fusion.1) | copy-start | bytes 3076
  69.5 8.6 %copy-start.30 = (bf16[2,2,2,3,128,128]{5,4,3,2,1,0:T(8,128)(2,1)S(1)}, bf16[2,2,2,3,128,128]{5,4,3,2,1,0:T(8,128)(2,1)}, u32[]{:S(2)}) copy-start(bf16[2,2,2,3,128,128]{5,4,3,2,1,0:T(8,128)(2,1)} %param.23) | copy-start | bytes 2359300
  69.5 3.9 %collective-permute-start = (bf16[2,384]{1,0:T(2,128)(2,1)S(1)}, bf16[2,384]{1,0:T(2,128)(2,1)S(1)}, u32[]{:S(2)}, u32[]{:S(2)}) collective-permute-start(bf16[2,384]{1,0:T(2,128)(2,1)S(1)} %get-tuple-element.353), channel_id=1, source_target_pairs={{0,4},{4,8},{8,12},{1,5},{5,9},{9,13},{2,6},{6,10},{10,14},{3,7},{... | collective-permute-start | bytes 4616 | tf_op jit(solution)/shard_map/ppermute | solution.py:18
  72.1 5.5 %collective-permute-start.1 = (bf16[2,384]{1,0:T(2,128)(2,1)S(1)}, bf16[2,384]{1,0:T(2,128)(2,1)S(1)}, u32[]{:S(2)}, u32[]{:S(2)}) collective-permute-start(bf16[2,384]{1,0:T(2,128)(2,1)S(1)} %get-tuple-element.354), channel_id=1, source_target_pairs={{4,0},{8,4},{12,8},{5,1},{9,5},{13,9},{6,2},{10,6},{14,10},{7,3},{... | collective-permute-start | bytes 4616 | tf_op jit(solution)/shard_map/ppermute | solution.py:20
  114.7 0.9 copy-start.23
  115.7 0.6 copy-start.22
  116.4 1.7 copy-start.3
  118.9 33.3 %copy-start = (bf16[256,2048]{1,0:T(8,128)(2,1)S(1)}, bf16[256,2048]{1,0:T(8,128)(2,1)}, u32[]{:S(2)}) copy-start(bf16[256,2048]{1,0:T(8,128)(2,1)} %all-gather.31.cloned.1.call-done) | copy-start | bytes 3145732
  118.9 33.3 %copy-start.10 = (f32[1,2048]{1,0:T(1,128)S(1)}, f32[1,2048]{1,0:T(1,128)}, u32[]{:S(2)}) copy-start(f32[1,2048]{1,0:T(1,128)} %copy-done.9) | copy-start | bytes 24580
  118.9 33.3 %copy-start.28 = (f32[256]{0:T(256)S(1)}, f32[256]{0:T(256)}, u32[]{:S(2)}) copy-start(f32[256]{0:T(256)} %copy-done.27) | copy-start | bytes 3076
  156.6 27.1 %copy-start.20 = (f32[384]{0:T(512)S(1)}, f32[384]{0:T(512)}, u32[]{:S(2)}) copy-start(f32[384]{0:T(512)} %get-tuple-element.273) | copy-start | bytes 4612
  156.6 27.2 %copy-start.21 = (f32[384]{0:T(512)S(1)}, f32[384]{0:T(512)}, u32[]{:S(2)}) copy-start(f32[384]{0:T(512)} %get-tuple-element.276) | copy-start | bytes 4612
  156.6 80.3 %copy-start.7 = (f32[1,2048]{1,0:T(1,128)S(1)}, f32[1,2048]{1,0:T(1,128)}, u32[]{:S(2)}) copy-start(f32[1,2048]{1,0:T(1,128)} %get-tuple-element.403) | copy-start | bytes 24580
  156.6 41.7 %all-gather.33.cloned.1.call-start = ((), (), s32[]{:S(2)}) async-start(), calls=%async_computation.4 | async-start | bytes 1310720 | tf_op jit(solution)/shard_map/all_gather | solution.py:75
  181.5 55.5 %all-gather.41.cloned.1.call-start = ((), (), s32[]{:S(2)}) async-start(), calls=%async_computation.9 | async-start | bytes 1966080 | tf_op jit(solution)/shard_map/all_gather | solution.py:79
  182.2 139.5 %all-gather.43.cloned.1.call-start = ((), (), s32[]{:S(2)}) async-start(), calls=%async_computation.10 | async-start | bytes 1966080 | tf_op jit(solution)/shard_map/all_gather | solution.py:84
  183.0 138.7 %all-gather.45.cloned.1.call-start = ((), (), s32[]{:S(2)}) async-start(), calls=%async_computation.11 | async-start | bytes 1966080 | tf_op jit(solution)/shard_map/all_gather | solution.py:141
  183.7 165.8 %reduce-scatter.5.cloned.1.call-start = ((), (), s32[]{:S(2)}) async-start(), calls=%async_computation.5 | async-start | bytes 1310720 | tf_op jit(solution)/shard_map/reduce_scatter | solution.py:144
  199.8 39.6 %copy-start.25 = (f32[256]{0:T(256)}, f32[256]{0:T(256)S(1)}, u32[]{:S(2)}) copy-start(f32[256]{0:T(256)S(1)} %add_rsqrt_fusion) | copy-start | bytes 3076
  236.9 10.7 %copy-start.11 = (f32[384]{0:T(512)S(1)}, f32[384]{0:T(512)}, u32[]{:S(2)}) copy-start(f32[384]{0:T(512)} %get-tuple-element.266) | copy-start | bytes 4612
  236.9 10.7 %copy-start.12 = (f32[384]{0:T(512)S(1)}, f32[384]{0:T(512)}, u32[]{:S(2)}) copy-start(f32[384]{0:T(512)} %get-tuple-element.271) | copy-start | bytes 4612
  236.9 10.7 %copy-start.13 = (f32[384]{0:T(512)S(1)}, f32[384]{0:T(512)}, u32[]{:S(2)}) copy-start(f32[384]{0:T(512)} %get-tuple-element.272) | copy-start | bytes 4612
  239.4 8.6 %copy-start.31 = (bf16[2,2,2,3,128,128]{5,4,3,2,1,0:T(8,128)(2,1)S(1)}, bf16[2,2,2,3,128,128]{5,4,3,2,1,0:T(8,128)(2,1)}, u32[]{:S(2)}) copy-start(bf16[2,2,2,3,128,128]{5,4,3,2,1,0:T(8,128)(2,1)} %param.23) | copy-start | bytes 2359300
  239.5 3.9 %collective-permute-start.2 = (bf16[2,384]{1,0:T(2,128)(2,1)S(1)}, bf16[2,384]{1,0:T(2,128)(2,1)S(1)}, u32[]{:S(2)}, u32[]{:S(2)}) collective-permute-start(bf16[2,384]{1,0:T(2,128)(2,1)S(1)} %get-tuple-element.341), channel_id=1, source_target_pairs={{0,4},{4,8},{8,12},{1,5},{5,9},{9,13},{2,6},{6,10},{10,14},{3,7},{... | collective-permute-start | bytes 4616 | tf_op jit(solution)/shard_map/ppermute | solution.py:18
  242.1 5.5 %collective-permute-start.3 = (bf16[2,384]{1,0:T(2,128)(2,1)S(1)}, bf16[2,384]{1,0:T(2,128)(2,1)S(1)}, u32[]{:S(2)}, u32[]{:S(2)}) collective-permute-start(bf16[2,384]{1,0:T(2,128)(2,1)S(1)} %get-tuple-element.342), channel_id=1, source_target_pairs={{4,0},{8,4},{12,8},{5,1},{9,5},{13,9},{6,2},{10,6},{14,10},{7,3},{... | collective-permute-start | bytes 4616 | tf_op jit(solution)/shard_map/ppermute | solution.py:20
  284.8 1.7 copy-start.4
  287.3 34.3 %copy-start.1 = (bf16[256,2048]{1,0:T(8,128)(2,1)S(1)}, bf16[256,2048]{1,0:T(8,128)(2,1)}, u32[]{:S(2)}) copy-start(bf16[256,2048]{1,0:T(8,128)(2,1)} %all-gather.33.cloned.1.call-done) | copy-start | bytes 3145732
  287.4 34.3 %copy-start.8 = (f32[1,2048]{1,0:T(1,128)S(1)}, f32[1,2048]{1,0:T(1,128)}, u32[]{:S(2)}) copy-start(f32[1,2048]{1,0:T(1,128)} %get-tuple-element.403) | copy-start | bytes 24580
  287.4 34.3 %copy-start.26 = (f32[256]{0:T(256)S(1)}, f32[256]{0:T(256)}, u32[]{:S(2)}) copy-start(f32[256]{0:T(256)} %copy-done.25) | copy-start | bytes 3076
  321.7 27.8 %copy-start.2 = (bf16[256,512]{1,0:T(8,128)(2,1)S(1)}, bf16[256,512]{1,0:T(8,128)(2,1)}, u32[]{:S(2)}) copy-start(bf16[256,512]{1,0:T(8,128)(2,1)} %add_convert_fusion.1) | copy-start | bytes 786436
Sparse Core Ops, SparseCore 0:
  8.9 19.4 all-gather.30
  29.9 37.0 all-gather.34
  68.5 36.0 all-gather.36
  106.0 36.0 all-gather.38
  156.7 22.8 reduce-scatter.2
  181.6 16.6 all-gather.32
  199.9 37.0 all-gather.40
  238.5 36.0 all-gather.42
  276.1 36.0 all-gather.44
  326.4 23.0 reduce-scatter.4
where the time goes:
time: 360 us; the launch traced here: 358 us
  waiting for transfers between devices  158 us (44%)
  blocking collectives  97.5 us (27%)
  local copies, waits for them, and re-layouts  35.6 us (10%)
  other arithmetic  24.8 us (7%)
  between operations  16.9 us (5%)
  matrix products  16.4 us (5%)
  starting transfers between devices  8.37 us (2%)
    all_gather x8, blocking collectives, carried_in(): gathered = jax.tree.map(lambda a: lax.all_gather(a, axis), part)  97.5 us
    all_gather x2, waiting for transfers between devices, local(): lax.all_gather(convolution_in_weight[layer_index], 'sp', axis=0, tiled=True)  74.2 us
    reduce_scatter x2, waiting for transfers between devices, local(): lax.psum_scatter(partials.astype(jnp.float32).astype(jnp.bfloat16), 'tp',...  46 us
    all_gather x2, waiting for transfers between devices, local(): features = lax.all_gather(stream, 'tp', axis=1, tiled=True)  27 us
    rev x4, local copies, waits for them, and re-layouts, local(): lax.associative_scan(combine_pairs, (jnp.exp(decay_logarithm), driven), r...  11.6 us
    slice x220, local copies, waits for them, and re-layouts, local(): lax.associative_scan(combine_pairs, (jnp.exp(decay_logarithm), driven), r...  10.5 us
    dot_general x2, matrix products, local(): jnp.dot(gated, lax.all_gather(output_weight[layer_index], 'sp', axis=1, t...  8.97 us
    ppermute x2, waiting for transfers between devices, extended(): lax.ppermute(head, axis, [((i + 1) % count, i) for i in range(ends)])  8.32 us
  transfers between devices with their start and end apart: 14, of which 8 were waited for; matrix products, arithmetic and copies ran while one was open for 18% of the time, Pallas kernels for 0%

commit v1 on v0

--- a/solution.py
+++ b/solution.py
@@ -72,7 +72,7 @@
     at_first = (positions == 0)[:, None]
     at_last = (positions == seq_length - 1)[:, None]
     for layer_index in range(convolution_in_weight.shape[0]):
-        features = lax.all_gather(stream, "tp", axis=1, tiled=True)
+        features = jnp.concatenate(lax.all_gather(stream, "tp"), axis=1)
         normed = rms_norm(features, layer_norm_gain[layer_index])
         acc_x = jnp.dot(
             normed,

time: 360 us -> 506 us (1.41)
  local copies, waits for them, and re-layouts: 35.6 us -> 132 us
  other arithmetic: 24.8 us -> 73.2 us
  matrix products: 16.4 us -> 22.9 us
    slice x220, local copies, waits for them, and re-layouts: 10.5 us -> 71.9 us  [local(): lax.associative_scan(combine_pairs, (jnp.exp(decay_logarithm), driven), r...]
    pad x112, local copies, waits for them, and re-layouts: 5.35 us -> 29.2 us  [local(): lax.associative_scan(combine_pairs, (jnp.exp(decay_logarithm), driven), r...]
    add x60, other arithmetic: 5.93 us -> 23.6 us  [local(): lax.associative_scan(combine_pairs, (jnp.exp(decay_logarithm), driven), r...]
    add x58, other arithmetic: 1.14 us -> 14.2 us  [combine_pairs(): return (earlier[0] * latter[0], latter[0] * earlier[1] + latter[1])]
    concatenate x56, other arithmetic: 1.96 us -> 14.1 us  [local(): lax.associative_scan(combine_pairs, (jnp.exp(decay_logarithm), driven), r...]
    all_gather x2, waiting for transfers between devices: 74.2 us -> 66.2 us  [local(): lax.all_gather(convolution_in_weight[layer_index], 'sp', axis=0, tiled=True)]
    convert_element_type x0 -> x4, other arithmetic: none -> 6.38 us  [the longest x2 5.7 us: rms_norm(): floats = values.astype(jnp.float32)]
  transfers between devices with their start and end apart: 14 -> 14, of which waited for: 8 -> 8; matrix products, arithmetic and copies ran while one was open for 18% -> 42% of each run, Pallas kernels for 0% -> 0%
where the time goes in v1:
time: 506 us; the launch traced here: 502 us
  waiting for transfers between devices  153 us (30%)
  local copies, waits for them, and re-layouts  132 us (26%)
  blocking collectives  96.2 us (19%)
  other arithmetic  73.2 us (14%)
  matrix products  22.9 us (5%)
  between operations  17 us (3%)
  starting transfers between devices  7.93 us (2%)
    all_gather x8, blocking collectives, carried_in(): gathered = jax.tree.map(lambda a: lax.all_gather(a, axis), part)  96.2 us
    slice x220, local copies, waits for them, and re-layouts, local(): lax.associative_scan(combine_pairs, (jnp.exp(decay_logarithm), driven), r...  71.9 us
    all_gather x2, waiting for transfers between devices, local(): lax.all_gather(convolution_in_weight[layer_index], 'sp', axis=0, tiled=True)  66.2 us
    reduce_scatter x2, waiting for transfers between devices, local(): lax.psum_scatter(partials.astype(jnp.float32).astype(jnp.bfloat16), 'tp',...  46.5 us
    pad x112, local copies, waits for them, and re-layouts, local(): lax.associative_scan(combine_pairs, (jnp.exp(decay_logarithm), driven), r...  29.2 us
    all_gather x2, waiting for transfers between devices, local(): features = jnp.concatenate(lax.all_gather(stream, 'tp'), axis=1)  28.7 us
    add x60, other arithmetic, local(): lax.associative_scan(combine_pairs, (jnp.exp(decay_logarithm), driven), r...  23.6 us
    add x58, other arithmetic, combine_pairs(): return (earlier[0] * latter[0], latter[0] * earlier[1] + latter[1])  14.2 us
  transfers between devices with their start and end apart: 14, of which 8 were waited for; matrix products, arithmetic and copies ran while one was open for 42% of the time, Pallas kernels for 0%

profile of v1, /device:TPU:0, one launch (start us, length us, event | category | flops | bytes accessed | tf_op | source)
XLA Modules:
  0.0 502.1 jit_solution(7490269021349649992)
XLA Ops:
  7.3 2.1 fusion.199
  14.2 14.1 %all-gather.33.cloned.1.call-done = bf16[1024,512]{1,0:T(8,128)(2,1)} async-done(((bf16[256,512]{1,0:T(8,128)(2,1)}), bf16[1024,512]{1,0:T(8,128)(2,1)}) %all-gather.33.cloned.1.call-update) | async-done | bytes 1048592 | tf_op jit(solution)/shard_map/all_gather | solution.py:75
  28.3 2.8 convert_bitcast_fusion
  31.2 2.0 copy.89
  33.9 33.1 %all-gather.35.cloned.1.call-done = bf16[1,2048,384]{2,1,0:T(8,128)(2,1)} async-done(((bf16[1,512,384]{2,1,0:T(8,128)(2,1)}), bf16[1,2048,384]{2,1,0:T(8,128)(2,1)}) %all-gather.35.cloned.1.call-update) | async-done | bytes 1572880 | tf_op jit(solution)/shard_map/all_gather | solution.py:79
  67.0 2.1 fusion.39
  69.1 2.5 collective-permute-start
  73.0 4.2 collective-permute-done.1
  85.3 2.1 convert_multiply_fusion.4
  123.5 12.3 %all-gather.17 = f32[4,1,384]{2,1,0:T(1,128)S(1)} all-gather(f32[1,1,384]{2,1,0:T(1,128)S(1)} %add_bitcast_fusion.6), channel_id=5, replica_groups=mesh['grp'=2,'sp'=4,'tp'=4] {'sp'}, dimensions={0}, use_global_device_ids=true | all-gather | bytes 7680 | tf_op jit(solution)/shard_map/all_gather | solution.py:31
  138.6 11.9 %all-gather.16 = f32[4,1,384]{2,1,0:T(1,128)S(1)} all-gather(f32[1,1,384]{2,1,0:T(1,128)S(1)} %add_bitcast_fusion.7), channel_id=4, replica_groups=mesh['grp'=2,'sp'=4,'tp'=4] {'sp'}, dimensions={0}, use_global_device_ids=true | all-gather | bytes 7680 | tf_op jit(solution)/shard_map/all_gather | solution.py:31
  159.5 2.0 pad.433
  172.4 2.4 slice.1256
  174.9 2.4 slice.1318
  182.9 1.8 fusion.119
  185.9 1.6 pad_maximum_fusion.3
  187.5 2.5 pad.454
  190.8 1.8 add.997
  193.3 11.9 %all-gather.19 = f32[4,1,384]{2,1,0:T(1,128)S(1)} all-gather(f32[1,1,384]{2,1,0:T(1,128)S(1)} %add_bitcast_fusion.4), channel_id=7, replica_groups=mesh['grp'=2,'sp'=4,'tp'=4] {'sp'}, dimensions={0}, use_global_device_ids=true | all-gather | bytes 7680 | tf_op jit(solution)/shard_map/all_gather | solution.py:31
  206.0 11.9 %all-gather.18 = f32[4,1,384]{2,1,0:T(1,128)S(1)} all-gather(f32[1,1,384]{2,1,0:T(1,128)S(1)} %add_bitcast_fusion.5), channel_id=6, replica_groups=mesh['grp'=2,'sp'=4,'tp'=4] {'sp'}, dimensions={0}, use_global_device_ids=true | all-gather | bytes 7680 | tf_op jit(solution)/shard_map/all_gather | solution.py:31
  218.2 2.6 rev.16
  220.8 2.6 rev.17
  223.4 4.4 convolution_convert_fusion.1
  227.9 23.2 %reduce-scatter.3.cloned.1.call-done = bf16[256,512]{1,0:T(8,128)(2,1)} async-done(((bf16[256,2048]{1,0:T(8,128)(2,1)}), bf16[256,512]{1,0:T(8,128)(2,1)}) %reduce-scatter.3.cloned.1.call-update) | async-done | bytes 262160 | tf_op jit(solution)/shard_map/reduce_scatter | solution.py:144
  251.2 1.8 add_convert_fusion.1
  255.3 14.5 %all-gather.41.cloned.1.call-done = bf16[1024,512]{1,0:T(8,128)(2,1)} async-done(((bf16[256,512]{1,0:T(8,128)(2,1)}), bf16[1024,512]{1,0:T(8,128)(2,1)}) %all-gather.41.cloned.1.call-update) | async-done | bytes 1048592 | tf_op jit(solution)/shard_map/all_gather | solution.py:75
  269.8 2.8 bitcast_convert_fusion
  272.7 2.0 copy.103
  275.4 33.1 %all-gather.43.cloned.1.call-done = bf16[1,2048,384]{2,1,0:T(8,128)(2,1)} async-done(((bf16[1,512,384]{2,1,0:T(8,128)(2,1)}), bf16[1,2048,384]{2,1,0:T(8,128)(2,1)}) %all-gather.43.cloned.1.call-update) | async-done | bytes 1572880 | tf_op jit(solution)/shard_map/all_gather | solution.py:79
  308.5 2.1 fusion.48
  310.6 2.5 collective-permute-start.2
  314.5 4.2 collective-permute-done.3
  326.9 2.1 convert_multiply_fusion.2
  365.4 12.4 %all-gather.21 = f32[4,1,384]{2,1,0:T(1,128)S(1)} all-gather(f32[1,1,384]{2,1,0:T(1,128)S(1)} %add_bitcast_fusion.2), channel_id=13, replica_groups=mesh['grp'=2,'sp'=4,'tp'=4] {'sp'}, dimensions={0}, use_global_device_ids=true | all-gather | bytes 7680 | tf_op jit(solution)/shard_map/all_gather | solution.py:31
  380.5 11.9 %all-gather.20 = f32[4,1,384]{2,1,0:T(1,128)S(1)} all-gather(f32[1,1,384]{2,1,0:T(1,128)S(1)} %add_bitcast_fusion.3), channel_id=12, replica_groups=mesh['grp'=2,'sp'=4,'tp'=4] {'sp'}, dimensions={0}, use_global_device_ids=true | all-gather | bytes 7680 | tf_op jit(solution)/shard_map/all_gather | solution.py:31
  401.7 2.0 pad.497
  414.7 2.4 slice.1436
  417.1 2.4 slice.1498
  425.1 1.8 fusion.117
  427.0 2.5 pad.519
  431.9 2.0 add.1085
  434.5 11.9 %all-gather.23 = f32[4,1,384]{2,1,0:T(1,128)S(1)} all-gather(f32[1,1,384]{2,1,0:T(1,128)S(1)} %add_bitcast_fusion), channel_id=15, replica_groups=mesh['grp'=2,'sp'=4,'tp'=4] {'sp'}, dimensions={0}, use_global_device_ids=true | all-gather | bytes 7680 | tf_op jit(solution)/shard_map/all_gather | solution.py:31
  447.2 11.9 %all-gather.22 = f32[4,1,384]{2,1,0:T(1,128)S(1)} all-gather(f32[1,1,384]{2,1,0:T(1,128)S(1)} %add_bitcast_fusion.1), channel_id=14, replica_groups=mesh['grp'=2,'sp'=4,'tp'=4] {'sp'}, dimensions={0}, use_global_device_ids=true | all-gather | bytes 7680 | tf_op jit(solution)/shard_map/all_gather | solution.py:31
  459.2 2.6 rev.18
  461.8 3.9 rev.19
  465.7 4.6 convolution_convert_fusion
  470.3 23.2 %reduce-scatter.5.cloned.1.call-done = bf16[256,512]{1,0:T(8,128)(2,1)} async-done(((bf16[256,2048]{1,0:T(8,128)(2,1)}), bf16[256,512]{1,0:T(8,128)(2,1)}) %reduce-scatter.5.cloned.1.call-update) | async-done | bytes 262160 | tf_op jit(solution)/shard_map/reduce_scatter | solution.py:144
  493.5 1.7 add_convert_fusion
  (822 shorter events, 162.4 us)
Async XLA Ops:
  6.5 21.8 %all-gather.33.cloned.1.call-start = ((), (), s32[]{:S(2)}) async-start(), calls=%async_computation.4 | async-start | bytes 1310720 | tf_op jit(solution)/shard_map/all_gather | solution.py:75
  7.3 59.7 %all-gather.35.cloned.1.call-start = ((), (), s32[]{:S(2)}) async-start(), calls=%async_computation.5 | async-start | bytes 1966080 | tf_op jit(solution)/shard_map/all_gather | solution.py:79
  9.4 214.0 %all-gather.37.cloned.1.call-start = ((), (), s32[]{:S(2)}) async-start(), calls=%async_computation.6 | async-start | bytes 1966080 | tf_op jit(solution)/shard_map/all_gather | solution.py:84
  10.5 212.9 %all-gather.39.cloned.1.call-start = ((), (), s32[]{:S(2)}) async-start(), calls=%async_computation.7 | async-start | bytes 1966080 | tf_op jit(solution)/shard_map/all_gather | solution.py:141
  11.6 239.5 %reduce-scatter.3.cloned.1.call-start = ((), (), s32[]{:S(2)}) async-start(), calls=%async_computation.2 | async-start | bytes 1310720 | tf_op jit(solution)/shard_map/reduce_scatter | solution.py:144
  13.6 71.7 %copy-start.113 = (pred[256]{0:T(512)(128)(4,1)}, pred[256]{0:T(512)(128)(4,1)S(1)}, u32[]{:S(2)}) copy-start(pred[256]{0:T(512)(128)(4,1)S(1)} %get-tuple-element.485) | copy-start | bytes 772
  13.6 71.7 %copy-start.115 = (pred[256]{0:T(512)(128)(4,1)}, pred[256]{0:T(512)(128)(4,1)S(1)}, u32[]{:S(2)}) copy-start(pred[256]{0:T(512)(128)(4,1)S(1)} %get-tuple-element.486) | copy-start | bytes 772
  69.1 3.8 collective-permute-start
  71.6 5.5 %collective-permute-start.1 = (bf16[2,384]{1,0:T(2,128)(2,1)S(1)}, bf16[2,384]{1,0:T(2,128)(2,1)S(1)}, u32[]{:S(2)}, u32[]{:S(2)}) collective-permute-start(bf16[2,384]{1,0:T(2,128)(2,1)S(1)} %get-tuple-element.354), channel_id=1, source_target_pairs={{4,0},{8,4},{12,8},{5,1},{9,5},{13,9},{6,2},{10,6},{14,10},{7,3},{... | collective-permute-start | bytes 4616 | tf_op jit(solution)/shard_map/ppermute | solution.py:20
  123.3 27.3 %copy-start.58 = (f32[2,384]{1,0:T(2,128)S(1)}, f32[2,384]{1,0:T(2,128)}, u32[]{:S(2)}) copy-start(f32[2,384]{1,0:T(2,128)} %pad_add_fusion.5) | copy-start | bytes 9220
  123.3 27.3 %copy-start.84 = (f32[1,384]{1,0:T(1,128)S(1)}, f32[1,384]{1,0:T(1,128)}, u32[]{:S(2)}) copy-start(f32[1,384]{1,0:T(1,128)} %get-tuple-element.447) | copy-start | bytes 4612
  123.3 27.3 %copy-start.85 = (f32[1,384]{1,0:T(1,128)S(1)}, f32[1,384]{1,0:T(1,128)}, u32[]{:S(2)}) copy-start(f32[1,384]{1,0:T(1,128)} %get-tuple-element.448) | copy-start | bytes 4612
  123.3 27.3 %copy-start.43 = (f32[3,384]{1,0:T(4,128)S(1)}, f32[3,384]{1,0:T(4,128)}, u32[]{:S(2)}) copy-start(f32[3,384]{1,0:T(4,128)} %slice.1290) | copy-start | bytes 13828
  123.3 27.3 %copy-start.44 = (f32[3,384]{1,0:T(4,128)S(1)}, f32[3,384]{1,0:T(4,128)}, u32[]{:S(2)}) copy-start(f32[3,384]{1,0:T(4,128)} %slice.1307) | copy-start | bytes 13828
  123.4 27.4 %copy-start.81 = (f32[1,384]{1,0:T(1,128)S(1)}, f32[1,384]{1,0:T(1,128)}, u32[]{:S(2)}) copy-start(f32[1,384]{1,0:T(1,128)} %slice.1607) | copy-start | bytes 4612
  123.4 27.4 %copy-start.79 = (f32[1,384]{1,0:T(1,128)S(1)}, f32[1,384]{1,0:T(1,128)}, u32[]{:S(2)}) copy-start(f32[1,384]{1,0:T(1,128)} %slice.1581) | copy-start | bytes 4612
  123.4 28.1 %copy-start.36 = (f32[7,384]{1,0:T(8,128)S(1)}, f32[7,384]{1,0:T(8,128)}, u32[]{:S(2)}) copy-start(f32[7,384]{1,0:T(8,128)} %slice.1284) | copy-start | bytes 32260
  123.4 28.1 %copy-start.37 = (f32[7,384]{1,0:T(8,128)S(1)}, f32[7,384]{1,0:T(8,128)}, u32[]{:S(2)}) copy-start(f32[7,384]{1,0:T(8,128)} %slice.1309) | copy-start | bytes 32260
  138.5 33.1 %copy-start.5 = (f32[256,384]{1,0:T(8,128)}, f32[256,384]{1,0:T(8,128)S(1)}, u32[]{:S(2)}) copy-start(f32[256,384]{1,0:T(8,128)S(1)} %pad.422) | copy-start | bytes 1179652
  190.8 32.6 %copy-start.6 = (f32[256,384]{1,0:T(8,128)S(1)}, f32[256,384]{1,0:T(8,128)}, u32[]{:S(2)}) copy-start(f32[256,384]{1,0:T(8,128)} %copy-done.5) | copy-start | bytes 1179652
  227.9 27.4 %copy-start.63 = (f32[384]{0:T(512)S(1)}, f32[384]{0:T(512)}, u32[]{:S(2)}) copy-start(f32[384]{0:T(512)} %get-tuple-element.273) | copy-start | bytes 4612
  227.9 27.4 %copy-start.64 = (f32[384]{0:T(512)S(1)}, f32[384]{0:T(512)}, u32[]{:S(2)}) copy-start(f32[384]{0:T(512)} %get-tuple-element.276) | copy-start | bytes 4612
  227.9 42.0 %all-gather.41.cloned.1.call-start = ((), (), s32[]{:S(2)}) async-start(), calls=%async_computation.8 | async-start | bytes 1310720 | tf_op jit(solution)/shard_map/all_gather | solution.py:75
  253.0 55.5 %all-gather.43.cloned.1.call-start = ((), (), s32[]{:S(2)}) async-start(), calls=%async_computation.9 | async-start | bytes 1966080 | tf_op jit(solution)/shard_map/all_gather | solution.py:79
  253.8 211.9 %all-gather.45.cloned.1.call-start = ((), (), s32[]{:S(2)}) async-start(), calls=%async_computation.10 | async-start | bytes 1966080 | tf_op jit(solution)/shard_map/all_gather | solution.py:84
  254.5 211.2 %all-gather.47.cloned.1.call-start = ((), (), s32[]{:S(2)}) async-start(), calls=%async_computation.11 | async-start | bytes 1966080 | tf_op jit(solution)/shard_map/all_gather | solution.py:141
  255.2 238.3 %reduce-scatter.5.cloned.1.call-start = ((), (), s32[]{:S(2)}) async-start(), calls=%async_computation.3 | async-start | bytes 1310720 | tf_op jit(solution)/shard_map/reduce_scatter | solution.py:144
  275.4 43.3 %copy-start.49 = (f32[384]{0:T(512)S(1)}, f32[384]{0:T(512)}, u32[]{:S(2)}) copy-start(f32[384]{0:T(512)} %get-tuple-element.265) | copy-start | bytes 4612
  275.4 43.3 %copy-start.50 = (f32[384]{0:T(512)S(1)}, f32[384]{0:T(512)}, u32[]{:S(2)}) copy-start(f32[384]{0:T(512)} %get-tuple-element.266) | copy-start | bytes 4612
  275.4 43.3 %copy-start.51 = (f32[384]{0:T(512)S(1)}, f32[384]{0:T(512)}, u32[]{:S(2)}) copy-start(f32[384]{0:T(512)} %get-tuple-element.271) | copy-start | bytes 4612
  275.4 43.3 %copy-start.52 = (f32[384]{0:T(512)S(1)}, f32[384]{0:T(512)}, u32[]{:S(2)}) copy-start(f32[384]{0:T(512)} %get-tuple-element.272) | copy-start | bytes 4612
  310.6 3.8 collective-permute-start.2
  313.1 5.5 %collective-permute-start.3 = (bf16[2,384]{1,0:T(2,128)(2,1)S(1)}, bf16[2,384]{1,0:T(2,128)(2,1)S(1)}, u32[]{:S(2)}, u32[]{:S(2)}) collective-permute-start(bf16[2,384]{1,0:T(2,128)(2,1)S(1)} %get-tuple-element.342), channel_id=1, source_target_pairs={{4,0},{8,4},{12,8},{5,1},{9,5},{13,9},{6,2},{10,6},{14,10},{7,3},{... | collective-permute-start | bytes 4616 | tf_op jit(solution)/shard_map/ppermute | solution.py:20
  365.2 27.4 %copy-start.86 = (f32[1,384]{1,0:T(1,128)S(1)}, f32[1,384]{1,0:T(1,128)}, u32[]{:S(2)}) copy-start(f32[1,384]{1,0:T(1,128)} %get-tuple-element.433) | copy-start | bytes 4612
  365.2 27.5 %copy-start.87 = (f32[1,384]{1,0:T(1,128)S(1)}, f32[1,384]{1,0:T(1,128)}, u32[]{:S(2)}) copy-start(f32[1,384]{1,0:T(1,128)} %get-tuple-element.434) | copy-start | bytes 4612
  365.2 27.5 %copy-start.55 = (f32[2,384]{1,0:T(2,128)S(1)}, f32[2,384]{1,0:T(2,128)}, u32[]{:S(2)}) copy-start(f32[2,384]{1,0:T(2,128)} %pad_add_fusion) | copy-start | bytes 9220
  365.2 27.5 %copy-start.57 = (f32[2,384]{1,0:T(2,128)S(1)}, f32[2,384]{1,0:T(2,128)}, u32[]{:S(2)}) copy-start(f32[2,384]{1,0:T(2,128)} %pad_add_fusion.1) | copy-start | bytes 9220
  365.2 27.5 %copy-start.82 = (f32[1,384]{1,0:T(1,128)S(1)}, f32[1,384]{1,0:T(1,128)}, u32[]{:S(2)}) copy-start(f32[1,384]{1,0:T(1,128)} %get-tuple-element.431) | copy-start | bytes 4612
  365.2 27.5 %copy-start.83 = (f32[1,384]{1,0:T(1,128)S(1)}, f32[1,384]{1,0:T(1,128)}, u32[]{:S(2)}) copy-start(f32[1,384]{1,0:T(1,128)} %get-tuple-element.432) | copy-start | bytes 4612
  365.2 27.6 %copy-start.41 = (f32[3,384]{1,0:T(4,128)S(1)}, f32[3,384]{1,0:T(4,128)}, u32[]{:S(2)}) copy-start(f32[3,384]{1,0:T(4,128)} %slice.1470) | copy-start | bytes 13828
  365.2 27.6 %copy-start.42 = (f32[3,384]{1,0:T(4,128)S(1)}, f32[3,384]{1,0:T(4,128)}, u32[]{:S(2)}) copy-start(f32[3,384]{1,0:T(4,128)} %slice.1487) | copy-start | bytes 13828
  365.2 27.6 %copy-start.80 = (f32[1,384]{1,0:T(1,128)S(1)}, f32[1,384]{1,0:T(1,128)}, u32[]{:S(2)}) copy-start(f32[1,384]{1,0:T(1,128)} %slice.1717) | copy-start | bytes 4612
  365.2 27.7 %copy-start.78 = (f32[1,384]{1,0:T(1,128)S(1)}, f32[1,384]{1,0:T(1,128)}, u32[]{:S(2)}) copy-start(f32[1,384]{1,0:T(1,128)} %slice.1691) | copy-start | bytes 4612
  365.2 28.3 %copy-start.34 = (f32[7,384]{1,0:T(8,128)S(1)}, f32[7,384]{1,0:T(8,128)}, u32[]{:S(2)}) copy-start(f32[7,384]{1,0:T(8,128)} %slice.1464) | copy-start | bytes 32260
  365.3 28.3 %copy-start.35 = (f32[7,384]{1,0:T(8,128)S(1)}, f32[7,384]{1,0:T(8,128)}, u32[]{:S(2)}) copy-start(f32[7,384]{1,0:T(8,128)} %slice.1489) | copy-start | bytes 32260
  380.5 33.4 %copy-start.3 = (f32[256,384]{1,0:T(8,128)}, f32[256,384]{1,0:T(8,128)S(1)}, u32[]{:S(2)}) copy-start(f32[256,384]{1,0:T(8,128)S(1)} %pad.486) | copy-start | bytes 1179652
  431.9 33.8 %copy-start.4 = (f32[256,384]{1,0:T(8,128)S(1)}, f32[256,384]{1,0:T(8,128)}, u32[]{:S(2)}) copy-start(f32[256,384]{1,0:T(8,128)} %copy-done.3) | copy-start | bytes 1179652
  465.7 27.8 %copy-start.2 = (bf16[256,512]{1,0:T(8,128)(2,1)S(1)}, bf16[256,512]{1,0:T(8,128)(2,1)}, u32[]{:S(2)}) copy-start(bf16[256,512]{1,0:T(8,128)(2,1)} %add_convert_fusion.1) | copy-start | bytes 786436
  (83 other events, 749.9 us)
Sparse Core Ops, SparseCore 0:
  8.9 19.4 all-gather.32
  29.9 37.0 all-gather.34
  68.5 35.8 all-gather.36
  105.9 35.9 all-gather.38
  228.0 23.1 reduce-scatter.2
  253.1 16.6 all-gather.40
  271.4 37.0 all-gather.42
  310.0 35.8 all-gather.44
  347.5 35.9 all-gather.46
  470.4 23.0 reduce-scatter.4
